TPU v7x, 32 devices: a whole 2x2x4 slice. The times are simulated.
32 devices in a mesh: sp: 4 (over z), fs: 4 (over y, x), tp: 2 (over core).
Axes of the slice: x: 2, y: 2, z: 4, core: 2. Of those that a mesh axis runs over, the one named last changes fastest.
Arguments:
- tokens: bfloat16 [2048, 2048], P(('fs', 'sp')), parts along dimension 0, may hold values from -6 to 6
- norm_gain: bfloat16 [2048], replicated, may hold values from 0.099609375 to 1.8984375
- query_down: bfloat16 [2048, 512], P('sp'), may hold values from -0.125 to 0.125
- query_gain: bfloat16 [512], replicated, may hold values from 0.099609375 to 1.8984375
- latent_down: bfloat16 [2048, 256], replicated, may hold values from -0.125 to 0.125
- latent_gain: bfloat16 [256], replicated, may hold values from 0.099609375 to 1.8984375
- rope_down: bfloat16 [2048, 64], replicated, may hold values from -30 to 30
- query_up: bfloat16 [512, 1536], P(None, 'tp'), may hold values from -0.25 to 0.25
- key_up: bfloat16 [256, 1024], P(None, 'tp'), may hold values from -0.75 to 0.75
- value_up: bfloat16 [256, 1024], P(None, 'tp'), may hold values from -0.375 to 0.375
- glu_value: bfloat16 [2048, 1024], P('sp', 'tp'), may hold values from -0.125 to 0.125
- glu_gate: bfloat16 [2048, 1024], P('sp', 'tp'), may hold values from -0.125 to 0.125
- conv_taps: bfloat16 [31, 1024], P(None, 'tp'), may hold values from -1 to 1
- group_gain: bfloat16 [1024], P('tp'), may hold values from 0.099609375 to 1.8984375
- head_proj: bfloat16 [1024, 2048], P('tp', 'sp'), may hold values from -0.75 to 0.75
- channel_proj: bfloat16 [1024, 2048], P('tp', 'sp'), may hold values from -0.1875 to 0.1875
Outputs:
- mixed_out: bfloat16 [2048, 2048], P(('fs', 'sp'), 'tp'), parts along dimension 0
- log_weight: float32 [8, 2048], P('tp', ('fs', 'sp')), parts along dimension 1
There are 4 independent parts, one for each index of `fs`. A program takes and returns all parts, laid end to end along the dimension named above; an argument that names none is the same for every part. Nothing has to cross between parts.
All inputs are finite; a program needn't handle non-finite values.
Results may differ from a plain program's by a relative error of at most 0.015.
The roundings to bfloat16 on the way count: a program that leaves them out, or rounds other values in their place, can miss the bound.
Values may be sent and summed in bfloat16 or wider, within the bound.
A program may use at most 128 MiB of HBM per device.

v0:
```python
import jax
import jax.numpy as jnp
from jax import lax
from jax.sharding import PartitionSpec as P

NOPE = 128
ROPE = 64
VDIM = 128
KVR = 256
CH = 1024
GROUPS = 8
GRID_W = 64
norm_eps = 1e-06
rope_base = 10000.0
far_below = -1e30


def padded_2(block, sides, width):
    for axis, dim in sides:
        count = lax.axis_size(axis)
        forward = [(i, i + 1) for i in range(count - 1)]
        backward = [(target, source) for source, target in forward]
        low = lax.ppermute(
            lax.slice_in_dim(block, block.shape[dim] - width, None, axis=dim), axis, forward
        )
        high = lax.ppermute(lax.slice_in_dim(block, 0, width, axis=dim), axis, backward)
        block = jnp.concatenate([low, block, high], axis=dim)
    return block


def rms_scale(values, scale_gain):
    inv_rms = lax.rsqrt(jnp.mean(values * values, axis=-1, keepdims=True) + norm_eps)
    return values * inv_rms * scale_gain.astype(jnp.float32)


def angles_for(positions, rope_size):
    quarter = rope_size // 4
    inverse = rope_base ** (-jnp.arange(quarter, dtype=jnp.float32) / quarter)
    grid_row = (positions // GRID_W).astype(jnp.float32)
    grid_col = (positions % GRID_W).astype(jnp.float32)
    return jnp.concatenate([grid_row[:, None] * inverse, grid_col[:, None] * inverse], axis=-1)


def rotate(values, angles):
    half_size = values.shape[-1] // 2
    front_half = values[..., :half_size]
    back_half = values[..., half_size:]
    cosine = jnp.cos(angles)
    sine_part = jnp.sin(angles)
    return jnp.concatenate(
        [front_half * cosine - back_half * sine_part, back_half * cosine + front_half * sine_part],
        axis=-1,
    )


def key_block(normed, latent_down, latent_gain, rope_down, positions):
    latent = jnp.dot(normed, latent_down, preferred_element_type=jnp.float32)
    latent = rms_scale(latent, latent_gain).astype(jnp.bfloat16)
    rope_key = jnp.dot(normed, rope_down, preferred_element_type=jnp.float32)
    rope_key = rotate(rope_key, angles_for(positions, rope_key.shape[-1])).astype(jnp.bfloat16)
    return jnp.concatenate([latent, rope_key], axis=1)


def per_device(
    tokens,
    norm_gain,
    query_down,
    query_gain,
    latent_down,
    latent_gain,
    rope_down,
    query_up,
    key_up,
    value_up,
    glu_value,
    glu_gate,
    conv_taps,
    group_gain,
    head_proj,
    channel_proj,
):
    tok_count = tokens.shape[0]
    reach_rows = conv_taps.shape[0] // 2
    head_count = key_up.shape[1] // NOPE
    normed = rms_scale(tokens.astype(jnp.float32), norm_gain).astype(jnp.bfloat16)
    offsets = lax.axis_index("sp") * tok_count + jnp.arange(tok_count, dtype=jnp.int32)
    query_latent = jnp.dot(
        normed,
        lax.all_gather(query_down, "sp", axis=0, tiled=True),
        preferred_element_type=jnp.float32,
    )
    value_in = jnp.dot(
        normed,
        lax.all_gather(glu_value, "sp", axis=0, tiled=True),
        preferred_element_type=jnp.float32,
    )
    gate_in = jnp.dot(
        normed,
        lax.all_gather(glu_gate, "sp", axis=0, tiled=True),
        preferred_element_type=jnp.float32,
    )
    latent_query = rms_scale(query_latent, query_gain).astype(jnp.bfloat16)
    query_all = jnp.dot(latent_query, query_up, preferred_element_type=jnp.float32).reshape(
        tok_count, head_count, NOPE + ROPE
    )
    query_plain = query_all[:, :, :NOPE].astype(jnp.bfloat16)
    query_rope = rotate(query_all[:, :, NOPE:], angles_for(offsets, ROPE)[:, None, :]).astype(
        jnp.bfloat16
    )
    absorbed = jnp.einsum(
        "thd,rhd->htr",
        query_plain,
        key_up.reshape(KVR, head_count, NOPE),
        preferred_element_type=jnp.float32,
    ).astype(jnp.bfloat16)
    queries = jnp.concatenate([absorbed, jnp.transpose(query_rope, (1, 0, 2))], axis=-1)
    score_scale = (NOPE + ROPE) ** (-0.5)
    half_rows = tok_count // lax.axis_size("tp")
    first_row = lax.axis_index("tp") * half_rows
    own_rows = lax.dynamic_slice_in_dim(normed, first_row, half_rows, 0)
    own_positions = lax.dynamic_slice_in_dim(offsets, first_row, half_rows, 0)
    own_keys = key_block(own_rows, latent_down, latent_gain, rope_down, own_positions)
    block_keys = lax.all_gather(own_keys, ("sp", "tp"), axis=0, tiled=True)
    row_max = jnp.full((head_count, tok_count), far_below, jnp.float32)
    scores = (
        jnp.einsum("hqc,kc->hqk", queries, block_keys, preferred_element_type=jnp.float32)
        * score_scale
    )
    new_max = jnp.maximum(row_max, jnp.max(scores, axis=2))
    weights = jnp.exp(scores - new_max[:, :, None])
    new_sum = jnp.sum(weights, axis=2)
    added = jnp.einsum(
        "hqk,kr->hqr",
        weights.astype(jnp.bfloat16),
        block_keys[:, :KVR],
        preferred_element_type=jnp.float32,
    )
    gated_rows = (value_in * jax.nn.sigmoid(gate_in)).astype(jnp.bfloat16)
    padded = padded_2(gated_rows, (("sp", 0),), reach_rows)
    filtered = padded[0:tok_count].astype(jnp.float32) * conv_taps[0].astype(jnp.float32)
    for tap_index in range(1, conv_taps.shape[0]):
        filtered = filtered + padded[tap_index : tap_index + tok_count].astype(
            jnp.float32
        ) * conv_taps[tap_index].astype(jnp.float32)
    grouped = filtered.reshape(tok_count, -1, CH // GROUPS)
    centred = grouped - jnp.mean(grouped, axis=-1, keepdims=True)
    spread = jnp.mean(centred * centred, axis=-1, keepdims=True)
    normal_groups = (centred * lax.rsqrt(spread + norm_eps)).reshape(tok_count, -1)
    conv_branch = jax.nn.silu(normal_groups * group_gain.astype(jnp.float32)).astype(jnp.bfloat16)
    attended = (added / new_sum[:, :, None]).astype(jnp.bfloat16)
    log_weight = new_max + jnp.log(new_sum)
    head_out = jnp.einsum(
        "htr,rhv->thv",
        attended,
        value_up.reshape(KVR, head_count, VDIM),
        preferred_element_type=jnp.float32,
    )
    head_out = head_out.reshape(tok_count, head_count * VDIM).astype(jnp.bfloat16)
    mixed_in = jnp.concatenate([head_out, conv_branch], axis=1)
    out_weight = jnp.concatenate([head_proj, channel_proj], axis=0)
    partial_terms = jnp.dot(
        mixed_in,
        lax.all_gather(out_weight, "sp", axis=1, tiled=True),
        preferred_element_type=jnp.float32,
    )
    mixed_out = lax.psum_scatter(
        partial_terms.astype(jnp.bfloat16), "tp", scatter_dimension=1, tiled=True
    )
    return (mixed_out, log_weight)


def solution(mesh):
    in_specs = (
        P(("fs", "sp"), None),
        P(),
        P("sp", None),
        P(),
        P(),
        P(),
        P(),
        P(None, "tp"),
        P(None, "tp"),
        P(None, "tp"),
        P("sp", "tp"),
        P("sp", "tp"),
        P(None, "tp"),
        P("tp"),
        P("tp", "sp"),
        P("tp", "sp"),
    )
    out_specs = (P(("fs", "sp"), "tp"), P("tp", ("fs", "sp")))
    return jax.shard_map(
        per_device, mesh=mesh, in_specs=in_specs, out_specs=out_specs, check_vma=False
    )
```

profile of v0, /device:TPU:0, one launch (start us, length us, event | category | flops | bytes accessed | tf_op | source)
XLA Modules:
  0.0 250.3 jit_solution(11534112967681167767)
XLA Ops:
  7.2 0.7 all-gather.7.cloned.1.call-update
  8.0 0.7 all-gather.9.cloned.1.call-update
  8.7 0.7 all-gather.5.cloned.1.call-update
  9.5 2.2 pad_maximum_fusion
  12.4 0.4 multiply_reduce_fusion.2
  13.2 0.6 convert_element_type.278
  14.0 0.2 fusion.26
  14.6 17.5 %all_gather.16 = bf16[512,320]{1,0:T(8,128)(2,1)S(1)} all-gather(bf16[64,320]{1,0:T(8,128)(2,1)S(1)} %pad_maximum_fusion.3), channel_id=1, replica_groups=mesh['sp'=4,'fs'=4,'tp'=2] {'sp','tp'}, dimensions={0}, use_global_device_ids=true | all-gather | bytes 368640 | tf_op jit(solution)/shard_map/all_gather | solution.py:123
  32.0 0.6 slice_convert_fusion.31
  32.7 0.7 slice_convert_fusion.32
  33.4 26.5 %all-gather.7.cloned.1.call-done = bf16[2048,512]{1,0:T(8,128)(2,1)} async-done(((bf16[512,512]{1,0:T(8,128)(2,1)}), bf16[2048,512]{1,0:T(8,128)(2,1)}) %all-gather.7.cloned.1.call-update) | async-done | bytes 2097168 | tf_op jit(solution)/shard_map/all_gather | solution.py:94
  59.8 2.0 fusion.75
  61.9 44.5 %all-gather.9.cloned.1.call-done = bf16[2048,512]{1,0:T(8,128)(2,1)} async-done(((bf16[512,512]{1,0:T(8,128)(2,1)}), bf16[2048,512]{1,0:T(8,128)(2,1)}) %all-gather.9.cloned.1.call-update) | async-done | bytes 2097168 | tf_op jit(solution)/shard_map/all_gather | solution.py:99
  106.4 2.1 fusion.6
  108.5 0.6 copy-done.6
  109.1 0.6 fusion.73
  109.7 2.7 %collective-permute-start = (bf16[15,512]{1,0:T(8,128)(2,1)}, bf16[15,512]{1,0:T(8,128)(2,1)}, u32[]{:S(2)}, u32[]{:S(2)}) collective-permute-start(bf16[15,512]{1,0:T(8,128)(2,1)} %get-tuple-element.6), channel_id=1, source_target_pairs={{0,8},{8,16},{16,24},{1,9},{9,17},{17,25},{2,10},{10,18},{18,26},{... | collective-permute-start | bytes 46088 | tf_op jit(solution)/shard_map/ppermute | solution.py:23
  112.4 1.3 collective-permute-start.1
  113.7 38.9 %all-gather.5.cloned.1.call-done = bf16[2048,512]{1,0:T(8,128)(2,1)} async-done(((bf16[512,512]{1,0:T(8,128)(2,1)}), bf16[2048,512]{1,0:T(8,128)(2,1)}) %all-gather.5.cloned.1.call-update) | async-done | bytes 2097168 | tf_op jit(solution)/shard_map/all_gather | solution.py:89
  152.6 2.1 multiply_reduce_fusion.1
  154.8 0.5 fusion.30
  155.3 0.3 convolution_convert_fusion.1
  155.6 0.6 fusion.74
  156.2 0.3 fusion.11
  156.8 0.6 fusion.7
  157.9 2.3 multiply_add_fusion
  160.3 0.2 reduce_sum.58
  160.5 0.4 multiply_reduce_fusion
  161.4 72.0 %all-gather.11.cloned.1.call-done = bf16[1024,2048]{1,0:T(8,128)(2,1)} async-done(((bf16[1024,512]{1,0:T(8,128)(2,1)}), bf16[1024,2048]{1,0:T(8,128)(2,1)}) %all-gather.11.cloned.1.call-update) | async-done | bytes 4194320 | tf_op jit(solution)/shard_map/all_gather | solution.py:163
  233.4 3.7 %convolution_convert_fusion = bf16[128,2048]{1,0:T(8,128)(2,1)} fusion(bf16[1024,2048]{1,0:T(8,128)(2,1)} %all-gather.11.cloned.1.call-done, bf16[128,512]{1,0:T(8,128)(2,1)S(1)} %multiply_convert_fusion, bf16[128,512]{1,0:T(8,128)(2,1)S(1)} %copy.28), kind=kOutput, calls=%fused_computation | convolution fusion | flops 537657344 | bytes 4980736 | tf_op jit(solution)/shard_map/dot_general | solution.py:161
  237.2 0.6 log_add_fusion
  237.8 6.0 %reduce-scatter.2.cloned.1.call-done = bf16[128,1024]{1,0:T(8,128)(2,1)} async-done(((bf16[128,2048]{1,0:T(8,128)(2,1)}), bf16[128,1024]{1,0:T(8,128)(2,1)}) %reduce-scatter.2.cloned.1.call-update) | async-done | bytes 262160 | tf_op jit(solution)/shard_map/reduce_scatter | solution.py:166
  (129 shorter events, 2.6 us)
Async XLA Ops:
  7.2 5.2 %copy-start = (bf16[2048,256]{1,0:T(8,128)(2,1)S(1)}, bf16[2048,256]{1,0:T(8,128)(2,1)}, u32[]{:S(2)}) copy-start(bf16[2048,256]{1,0:T(8,128)(2,1)} %param.20) | copy-start | bytes 3145732
  7.2 52.6 %all-gather.7.cloned.1.call-start = ((), (), s32[]{:S(2)}) async-start(), calls=%async_computation.2 | async-start | bytes 2621440 | tf_op jit(solution)/shard_map/all_gather | solution.py:94
  7.9 4.0 %copy-start.41 = (bf16[2048]{0:T(1024)(128)(2,1)S(1)}, bf16[2048]{0:T(1024)(128)(2,1)}, u32[]{:S(2)}) copy-start(bf16[2048]{0:T(1024)(128)(2,1)} %param.17) | copy-start | bytes 12292
  7.9 4.0 %copy-start.1 = (bf16[128,2048]{1,0:T(8,128)(2,1)S(1)}, bf16[128,2048]{1,0:T(8,128)(2,1)}, u32[]{:S(2)}) copy-start(bf16[128,2048]{1,0:T(8,128)(2,1)} %param.16) | copy-start | bytes 1572868
  7.9 98.4 %all-gather.9.cloned.1.call-start = ((), (), s32[]{:S(2)}) async-start(), calls=%async_computation.3 | async-start | bytes 2621440 | tf_op jit(solution)/shard_map/all_gather | solution.py:99
  8.7 143.9 %all-gather.5.cloned.1.call-start = ((), (), s32[]{:S(2)}) async-start(), calls=%async_computation.1 | async-start | bytes 2621440 | tf_op jit(solution)/shard_map/all_gather | solution.py:89
  9.4 224.0 %all-gather.11.cloned.1.call-start = ((), (), s32[]{:S(2)}) async-start(), calls=%async_computation.4 | async-start | bytes 5242880 | tf_op jit(solution)/shard_map/all_gather | solution.py:163
  11.7 1.2 copy-start.44
  11.7 1.2 copy-start.42
  11.7 1.2 copy-start.4
  11.7 1.4 copy-start.5
  11.7 1.5 copy-start.43
  11.7 232.0 %reduce-scatter.2.cloned.1.call-start = ((), (), s32[]{:S(2)}) async-start(), calls=%async_computation.5 | async-start | bytes 786432 | tf_op jit(solution)/shard_map/reduce_scatter | solution.py:166
  11.9 2.1 copy-start.3
  12.4 19.7 %copy-start.8 = (bf16[31,512]{1,0:T(8,128)(2,1)S(1)}, bf16[31,512]{1,0:T(8,128)(2,1)}, u32[]{:S(2)}) copy-start(bf16[31,512]{1,0:T(8,128)(2,1)} %param.28) | copy-start | bytes 95236
  109.1 45.6 %copy-start.2 = (bf16[512,768]{1,0:T(8,128)(2,1)S(1)}, bf16[512,768]{1,0:T(8,128)(2,1)}, u32[]{:S(2)}) copy-start(bf16[512,768]{1,0:T(8,128)(2,1)} %param.23) | copy-start | bytes 2359300
  109.7 47.8 %collective-permute-start = (bf16[15,512]{1,0:T(8,128)(2,1)}, bf16[15,512]{1,0:T(8,128)(2,1)}, u32[]{:S(2)}, u32[]{:S(2)}) collective-permute-start(bf16[15,512]{1,0:T(8,128)(2,1)} %get-tuple-element.6), channel_id=1, source_target_pairs={{0,8},{8,16},{16,24},{1,9},{9,17},{17,25},{2,10},{10,18},{18,26},{... | collective-permute-start | bytes 46088 | tf_op jit(solution)/shard_map/ppermute | solution.py:23
  112.4 45.1 %collective-permute-start.1 = (bf16[15,512]{1,0:T(8,128)(2,1)}, bf16[15,512]{1,0:T(8,128)(2,1)}, u32[]{:S(2)}, u32[]{:S(2)}) collective-permute-start(bf16[15,512]{1,0:T(8,128)(2,1)} %get-tuple-element.7), channel_id=1, source_target_pairs={{8,0},{16,8},{24,16},{9,1},{17,9},{25,17},{10,2},{18,10},{26,18},{... | collective-permute-start | bytes 46088 | tf_op jit(solution)/shard_map/ppermute | solution.py:26
  156.5 1.0 copy-start.7
  156.5 1.0 copy-start.9
  156.5 1.0 copy-start.10
  156.5 1.0 copy-start.11
  156.5 1.0 copy-start.12
  156.6 1.0 copy-start.13
  156.6 1.0 copy-start.14
  156.6 1.0 copy-start.15
  156.6 1.0 copy-start.16
  156.6 1.0 copy-start.17
  156.6 1.0 copy-start.18
  156.6 1.0 copy-start.19
  156.6 1.0 copy-start.20
  157.4 3.9 %copy-start.40 = (f32[512]{0:T(512)S(1)}, f32[512]{0:T(512)}, u32[]{:S(2)}) copy-start(f32[512]{0:T(512)} %convert_element_type.278) | copy-start | bytes 6148
  (20 other events, 20.2 us)
Sparse Core Ops, SparseCore 0:
  9.6 50.2 all-gather.6
  61.4 44.9 all-gather.8
  107.9 44.6 all-gather.4
  154.0 79.3 all-gather.10
  237.3 6.3 reduce-scatter.1
where the time goes:
time: 251 us; the launch traced here: 250 us
  waiting for transfers between devices  190 us (76%)
  blocking collectives  17.5 us (7%)
  between operations  14.7 us (6%)
  matrix products  12.5 us (5%)
  other arithmetic  9.21 us (4%)
  starting transfers between devices  4.14 us (2%)
    all_gather x1, waiting for transfers between devices, per_device(): lax.all_gather(out_weight, 'sp', axis=1, tiled=True)  72 us
    all_gather x1, waiting for transfers between devices, per_device(): lax.all_gather(glu_gate, 'sp', axis=0, tiled=True)  44.5 us
    all_gather x1, waiting for transfers between devices, per_device(): lax.all_gather(query_down, 'sp', axis=0, tiled=True)  38.9 us
    all_gather x1, waiting for transfers between devices, per_device(): lax.all_gather(glu_value, 'sp', axis=0, tiled=True)  26.5 us
    all_gather x1, blocking collectives, per_device(): block_keys = lax.all_gather(own_keys, ('sp', 'tp'), axis=0, tiled=True)  17.5 us
    reduce_scatter x1, waiting for transfers between devices, per_device(): lax.psum_scatter(partial_terms.astype(jnp.bfloat16), 'tp', scatter_dimens...  5.98 us
  transfers between devices with their start and end apart: 7, of which 5 were waited for; matrix products, arithmetic and copies ran while one was open for 8% of the time, Pallas kernels for 0%

commit v1 on v0

--- a/solution.py
+++ b/solution.py
@@ -160,7 +160,7 @@
     out_weight = jnp.concatenate([head_proj, channel_proj], axis=0)
     partial_terms = jnp.dot(
         mixed_in,
-        lax.all_gather(out_weight, "sp", axis=1, tiled=True),
+        jnp.concatenate(lax.all_gather(out_weight, "sp"), axis=1),
         preferred_element_type=jnp.float32,
     )
     mixed_out = lax.psum_scatter(

time: 251 us -> 259 us (1.032)
  local copies, waits for them, and re-layouts: 2.34 us -> 9.02 us
  waiting for transfers between devices: 190 us -> 187 us
    reshape x1, local copies, waits for them, and re-layouts: 0.14 us -> 6.31 us  [per_device(): jnp.concatenate(lax.all_gather(out_weight, 'sp'), axis=1)]
where the time goes in v1:
time: 259 us; the launch traced here: 258 us
  waiting for transfers between devices  187 us (72%)
  blocking collectives  17.5 us (7%)
  between operations  14.7 us (6%)
  matrix products  14.2 us (5%)
  other arithmetic  9.3 us (4%)
  local copies, waits for them, and re-layouts  9.02 us (3%)
  starting transfers between devices  6.62 us (3%)
    all_gather x1, waiting for transfers between devices, per_device(): lax.all_gather(out_weight, 'sp')  70.9 us
    all_gather x1, waiting for transfers between devices, per_device(): lax.all_gather(glu_gate, 'sp', axis=0, tiled=True)  45 us
    all_gather x1, waiting for transfers between devices, per_device(): lax.all_gather(query_down, 'sp', axis=0, tiled=True)  36.9 us
    all_gather x1, waiting for transfers between devices, per_device(): lax.all_gather(glu_value, 'sp', axis=0, tiled=True)  25.8 us
    all_gather x1, blocking collectives, per_device(): block_keys = lax.all_gather(own_keys, ('sp', 'tp'), axis=0, tiled=True)  17.5 us
    reshape x1, local copies, waits for them, and re-layouts, per_device(): jnp.concatenate(lax.all_gather(out_weight, 'sp'), axis=1)  6.31 us
    reduce_scatter x1, waiting for transfers between devices, per_device(): lax.psum_scatter(partial_terms.astype(jnp.bfloat16), 'tp', scatter_dimens...  5.98 us
  transfers between devices with their start and end apart: 7, of which 5 were waited for; matrix products, arithmetic and copies ran while one was open for 8% of the time, Pallas kernels for 0%

profile of v1, /device:TPU:0, one launch (start us, length us, event | category | flops | bytes accessed | tf_op | source)
XLA Modules:
  0.0 258.0 jit_solution(8051273998710876966)
XLA Ops:
  7.2 0.7 all-gather.8.cloned.1.call-update
  8.0 0.7 all-gather.10.cloned.1.call-update
  8.8 0.7 all-gather.6.cloned.1.call-update
  9.5 2.2 pad_maximum_fusion
  12.1 0.5 convert_element_type.278
  12.7 0.8 copy.70
  13.8 0.4 multiply_reduce_fusion.2
  14.7 0.2 fusion.28
  15.3 17.5 %all_gather.19 = bf16[512,320]{1,0:T(8,128)(2,1)S(1)} all-gather(bf16[64,320]{1,0:T(8,128)(2,1)S(1)} %pad_maximum_fusion.3), channel_id=1, replica_groups=mesh['sp'=4,'fs'=4,'tp'=2] {'sp','tp'}, dimensions={0}, use_global_device_ids=true | all-gather | bytes 368640 | tf_op jit(solution)/shard_map/all_gather | solution.py:123
  32.8 0.6 slice_convert_fusion.31
  33.5 0.7 slice_convert_fusion.32
  34.1 25.8 %all-gather.8.cloned.1.call-done = bf16[2048,512]{1,0:T(8,128)(2,1)} async-done(((bf16[512,512]{1,0:T(8,128)(2,1)}), bf16[2048,512]{1,0:T(8,128)(2,1)}) %all-gather.8.cloned.1.call-update) | async-done | bytes 2097168 | tf_op jit(solution)/shard_map/all_gather | solution.py:94
  60.0 2.0 fusion.78
  62.0 45.0 %all-gather.10.cloned.1.call-done = bf16[2048,512]{1,0:T(8,128)(2,1)} async-done(((bf16[512,512]{1,0:T(8,128)(2,1)}), bf16[2048,512]{1,0:T(8,128)(2,1)}) %all-gather.10.cloned.1.call-update) | async-done | bytes 2097168 | tf_op jit(solution)/shard_map/all_gather | solution.py:99
  107.0 2.1 fusion.6
  109.1 0.6 fusion.76
  109.7 1.3 collective-permute-start.1
  111.0 5.1 %collective-permute-start = (bf16[15,512]{1,0:T(8,128)(2,1)}, bf16[15,512]{1,0:T(8,128)(2,1)}, u32[]{:S(2)}, u32[]{:S(2)}) collective-permute-start(bf16[15,512]{1,0:T(8,128)(2,1)} %get-tuple-element.8), channel_id=1, source_target_pairs={{0,8},{8,16},{16,24},{1,9},{9,17},{17,25},{2,10},{10,18},{18,26},{... | collective-permute-start | bytes 46088 | tf_op jit(solution)/shard_map/ppermute | solution.py:23
  116.1 36.9 %all-gather.6.cloned.1.call-done = bf16[2048,512]{1,0:T(8,128)(2,1)} async-done(((bf16[512,512]{1,0:T(8,128)(2,1)}), bf16[2048,512]{1,0:T(8,128)(2,1)}) %all-gather.6.cloned.1.call-update) | async-done | bytes 2097168 | tf_op jit(solution)/shard_map/all_gather | solution.py:89
  153.0 2.1 multiply_reduce_fusion.1
  155.2 0.5 fusion.32
  156.2 1.2 convolution_convert_fusion.1
  157.4 0.6 fusion.77
  158.0 0.3 fusion.11
  158.6 0.6 fusion.7
  159.6 2.3 multiply_add_fusion
  162.2 0.4 multiply_reduce_fusion
  163.2 70.9 %all-gather.12.cloned.1.call-done = bf16[4096,512]{1,0:T(8,128)(2,1)} async-done(((bf16[1024,512]{1,0:T(8,128)(2,1)}), bf16[4096,512]{1,0:T(8,128)(2,1)}) %all-gather.12.cloned.1.call-update) | async-done | bytes 4194320 | tf_op jit(solution)/shard_map/all_gather | solution.py:163
  234.0 6.3 %copy.65 = bf16[1024,4,512]{0,2,1:T(8,128)(2,1)} copy(bf16[1024,4,512]{2,0,1:T(8,128)(2,1)} %bitcast.84) | data formatting | bytes 8388608 | tf_op jit(solution)/shard_map/reshape | solution.py:163
  240.4 4.5 %convolution_convert_fusion = bf16[128,2048]{1,0:T(8,128)(2,1)} fusion(bf16[1024,2048]{0,1:T(8,128)(2,1)} %bitcast.83, bf16[128,512]{1,0:T(8,128)(2,1)S(1)} %multiply_convert_fusion, bf16[128,512]{1,0:T(8,128)(2,1)S(1)} %copy.64), kind=kOutput, calls=%fused_computation | convolution fusion | flops 537657344 | bytes 4980736 | tf_op jit(solution)/shard_map/dot_general | solution.py:161
  244.9 0.6 log_add_fusion
  245.5 6.0 %reduce-scatter.2.cloned.1.call-done = bf16[128,1024]{1,0:T(8,128)(2,1)} async-done(((bf16[128,2048]{1,0:T(8,128)(2,1)}), bf16[128,1024]{1,0:T(8,128)(2,1)}) %reduce-scatter.2.cloned.1.call-update) | async-done | bytes 262160 | tf_op jit(solution)/shard_map/reduce_scatter | solution.py:166
  (130 shorter events, 3.2 us)
Async XLA Ops:
  7.2 6.6 %copy-start = (bf16[2048,256]{1,0:T(8,128)(2,1)S(1)}, bf16[2048,256]{1,0:T(8,128)(2,1)}, u32[]{:S(2)}) copy-start(bf16[2048,256]{1,0:T(8,128)(2,1)} %param.20) | copy-start | bytes 3145732
  7.2 52.8 %all-gather.8.cloned.1.call-start = ((), (), s32[]{:S(2)}) async-start(), calls=%async_computation.2 | async-start | bytes 2621440 | tf_op jit(solution)/shard_map/all_gather | solution.py:94
  7.9 4.0 %copy-start.39 = (bf16[2048]{0:T(1024)(128)(2,1)S(1)}, bf16[2048]{0:T(1024)(128)(2,1)}, u32[]{:S(2)}) copy-start(bf16[2048]{0:T(1024)(128)(2,1)} %param.17) | copy-start | bytes 12292
  7.9 4.0 %copy-start.1 = (bf16[128,2048]{1,0:T(8,128)(2,1)S(1)}, bf16[128,2048]{1,0:T(8,128)(2,1)}, u32[]{:S(2)}) copy-start(bf16[128,2048]{1,0:T(8,128)(2,1)} %param.16) | copy-start | bytes 1572868
  7.9 99.0 %all-gather.10.cloned.1.call-start = ((), (), s32[]{:S(2)}) async-start(), calls=%async_computation.3 | async-start | bytes 2621440 | tf_op jit(solution)/shard_map/all_gather | solution.py:99
  8.7 3.4 %copy-start.40 = (bf16[512]{0:T(512)(128)(2,1)S(1)}, bf16[512]{0:T(512)(128)(2,1)}, u32[]{:S(2)}) copy-start(bf16[512]{0:T(512)(128)(2,1)} %param.29) | copy-start | bytes 3076
  8.7 4.0 %copy-start.4 = (bf16[256,512]{1,0:T(8,128)(2,1)S(1)}, bf16[256,512]{1,0:T(8,128)(2,1)}, u32[]{:S(2)}) copy-start(bf16[256,512]{1,0:T(8,128)(2,1)} %param.25) | copy-start | bytes 786436
  8.7 144.3 %all-gather.6.cloned.1.call-start = ((), (), s32[]{:S(2)}) async-start(), calls=%async_computation.1 | async-start | bytes 2621440 | tf_op jit(solution)/shard_map/all_gather | solution.py:89
  9.4 4.2 %copy-start.42 = (bf16[256]{0:T(256)(128)(2,1)S(1)}, bf16[256]{0:T(256)(128)(2,1)}, u32[]{:S(2)}) copy-start(bf16[256]{0:T(256)(128)(2,1)} %param.21) | copy-start | bytes 1540
  9.4 224.6 %all-gather.12.cloned.1.call-start = ((), (), s32[]{:S(2)}) async-start(), calls=%async_computation.5 | async-start | bytes 5242880 | tf_op jit(solution)/shard_map/all_gather | solution.py:163
  11.7 2.5 copy-start.41
  11.8 2.9 %copy-start.3 = (bf16[2048,64]{0,1:T(8,128)(2,1)S(1)}, bf16[2048,64]{0,1:T(8,128)(2,1)}, u32[]{:S(2)}) copy-start(bf16[2048,64]{0,1:T(8,128)(2,1)} %param.22) | copy-start | bytes 786436
  11.8 239.7 %reduce-scatter.2.cloned.1.call-start = ((), (), s32[]{:S(2)}) async-start(), calls=%async_computation.4 | async-start | bytes 786432 | tf_op jit(solution)/shard_map/reduce_scatter | solution.py:166
  13.5 19.3 %copy-start.6 = (bf16[31,512]{1,0:T(8,128)(2,1)S(1)}, bf16[31,512]{1,0:T(8,128)(2,1)}, u32[]{:S(2)}) copy-start(bf16[31,512]{1,0:T(8,128)(2,1)} %param.28) | copy-start | bytes 95236
  109.1 46.1 %copy-start.2 = (bf16[512,768]{1,0:T(8,128)(2,1)S(1)}, bf16[512,768]{1,0:T(8,128)(2,1)}, u32[]{:S(2)}) copy-start(bf16[512,768]{1,0:T(8,128)(2,1)} %param.23) | copy-start | bytes 2359300
  109.7 49.6 %collective-permute-start.1 = (bf16[15,512]{1,0:T(8,128)(2,1)}, bf16[15,512]{1,0:T(8,128)(2,1)S(1)}, u32[]{:S(2)}, u32[]{:S(2)}) collective-permute-start(bf16[15,512]{1,0:T(8,128)(2,1)} %get-tuple-element.9), channel_id=1, source_target_pairs={{8,0},{16,8},{24,16},{9,1},{17,9},{25,17},{10,2},{18,10},{26,18},{... | collective-permute-start | bytes 46088 | tf_op jit(solution)/shard_map/ppermute | solution.py:26
  111.0 48.4 %collective-permute-start = (bf16[15,512]{1,0:T(8,128)(2,1)}, bf16[15,512]{1,0:T(8,128)(2,1)}, u32[]{:S(2)}, u32[]{:S(2)}) collective-permute-start(bf16[15,512]{1,0:T(8,128)(2,1)} %get-tuple-element.8), channel_id=1, source_target_pairs={{0,8},{8,16},{16,24},{1,9},{9,17},{17,25},{2,10},{10,18},{18,26},{... | collective-permute-start | bytes 46088 | tf_op jit(solution)/shard_map/ppermute | solution.py:23
  156.1 2.6 copy-start.5
  158.3 1.0 copy-start.7
  158.3 1.0 copy-start.8
  158.3 1.0 copy-start.9
  158.3 1.0 copy-start.10
  158.4 1.0 copy-start.11
  158.4 1.0 copy-start.12
  158.4 1.0 copy-start.13
  158.4 1.0 copy-start.14
  158.4 1.0 copy-start.15
  158.4 1.0 copy-start.16
  158.4 1.0 copy-start.17
  158.4 1.0 copy-start.18
  158.4 1.0 copy-start.19
  159.2 3.9 %copy-start.38 = (f32[512]{0:T(512)S(1)}, f32[512]{0:T(512)}, u32[]{:S(2)}) copy-start(f32[512]{0:T(512)} %convert_element_type.278) | copy-start | bytes 6148
  (18 other events, 18.5 us)
Sparse Core Ops, SparseCore 0:
  9.6 50.3 all-gather.7
  61.5 45.4 all-gather.9
  108.5 44.4 all-gather.5
  154.5 79.5 all-gather.11
  245.0 6.3 reduce-scatter.1
